TPU v7x, 1024 devices: a whole 4x8x16 slice. The times are simulated.
1024 devices in a mesh: ep: 32 (over z, core), tp: 32 (over y, x).
Axes of the slice: x: 4, y: 8, z: 16, core: 2. Of those that a mesh axis runs over, the one named last changes fastest.
Arguments:
- stream: bfloat16 [512, 4096], P('ep'), may hold values from -6 to 6
- previous_state: float32 [512, 128, 4096], P('ep', None, 'tp'), may hold values from -6 to 6
- mixer_norm_gain: float32 [4096], replicated, may hold values from 0.1 to 1.9
- query_matrix: bfloat16 [4096, 2048], P('ep'), may hold values from -0.09375 to 0.09375
- key_matrix: bfloat16 [4096, 2048], P('ep'), may hold values from -0.09375 to 0.09375
- value_matrix: bfloat16 [4096, 4096], P('ep', 'tp'), may hold values from -0.09375 to 0.09375
- output_gate_weight: bfloat16 [4096, 4096], P('ep', 'tp'), may hold values from -0.09375 to 0.09375
- decay_lower_factor: bfloat16 [4096, 64], replicated, may hold values from -0.09375 to 0.09375
- decay_upper_factor: bfloat16 [64, 2048], replicated, may hold values from -3 to 3
- forgetting_boost: float32 [512, 2048], P('ep'), may hold values from 0.02 to 1.5
- head_norm_gain: float32 [256], replicated, may hold values from 0.1 to 1.9
- output_matrix: bfloat16 [4096, 4096], P('tp'), may hold values from -0.1875 to 0.1875
- mixture_norm_gain: float32 [4096], replicated, may hold values from 0.1 to 1.9
- expert_gate_weight: bfloat16 [32, 1024, 4096], P('ep', 'tp'), may hold values from -0.09375 to 0.09375
- expert_up_weight: bfloat16 [32, 1024, 4096], P('ep', 'tp'), may hold values from -0.09375 to 0.09375
- expert_down_weight: bfloat16 [32, 1024, 4096], P('ep', None, 'tp'), may hold values from -0.375 to 0.375
- expert_index_table: int32 [512, 2], P('ep'), may hold values from 0 to 31, as said below
- expert_scores_within: float32 [512, 2], P('ep'), may hold values from -6 to 6
- group_probability: float32 [512], P('ep'), may hold values from 0.3 to 1
Outputs:
- new_stream: bfloat16 [512, 4096], P('ep', 'tp')
- new_state: float32 [512, 128, 4096], P('ep', None, 'tp')
Inputs may be any that keep to these rules, and one draw needn't show every extreme that they name: `expert_index_table`: the 2 experts of a sequence are distinct and lie in one group of 8 consecutive experts. Among the 16 sequences of one index of ep (aligned blocks of rows), each expert is named at most 2 times, and in every block some experts are named exactly 2 times.
All inputs are finite; a program needn't handle non-finite values.
Results may differ from a plain program's by a relative error of at most 0.02.
Values may be sent and summed in bfloat16 or wider, within the bound.
A program may use at most 32 MiB of HBM per device.

v0:
```python
import jax
import jax.numpy as jnp
from jax import lax
from jax.sharding import Mesh
from jax.sharding import PartitionSpec as P

HEAD_TOTAL = 16
KEY_CHANNELS = 128
DV = 256
TP = ("tp_0", "tp_1")


epsilon = 1e-06
forgetting_softness = 16.0


def split_up(value, dim, length):
    before, after = (value.shape[:dim], value.shape[dim + 1 :])
    return jnp.moveaxis(value.reshape(*before, length, -1, *after), dim, 0)


def sent_and_summed(value, axis, dim):
    tiles = split_up(value, dim, lax.axis_size(axis))
    arrived = lax.all_to_all(tiles, axis, split_axis=0, concat_axis=0, tiled=True)
    return arrived.sum(axis=0)


def from_everyone(value, axis):
    length = lax.axis_size(axis)
    return lax.all_to_all(
        jnp.broadcast_to(value[None], (length, *value.shape)), axis, 0, 0, tiled=True
    )


def of_everyone(value, axis):
    return from_everyone(value, axis).sum(axis=0)


def rows_for(lines, length):
    spare = -len(lines) % length
    return jnp.pad(lines, [(0, spare)] + [(0, 0)] * (lines.ndim - 1))


def reduced_to_own(tiles, axes, sequence):
    dims = [lax.axis_size(a) for a in axes]
    tiles = tiles.reshape(*dims, *tiles.shape[1:])
    tiles = tiles.transpose(*sequence, *range(len(axes), tiles.ndim))
    tiles = tiles.reshape(-1, *tiles.shape[len(axes) :])
    for k in sequence:
        tiles = lax.psum_scatter(tiles, axes[k], scatter_dimension=0, tiled=True)
    return tiles[0]


def stacked_from(value, axes, sequence):
    tiles = value
    for k in sequence:
        tiles = lax.all_gather(tiles, axes[k])
    done = sequence[::-1]
    back = [done.index(k) for k in range(len(axes))]
    tiles = tiles.transpose(*back, *range(len(axes), tiles.ndim))
    return tiles.reshape(-1, *value.shape)


def sum_by_parts(value, axes, sequence):
    length, lines = (lax.axis_size(axes), value.reshape(-1, *value.shape[1:][-1:]))
    tiles = rows_for(lines, length).reshape(length, -1, *lines.shape[1:])
    own = reduced_to_own(tiles, axes, sequence)
    whole = stacked_from(own, axes, sequence[::-1]).reshape(-1, *lines.shape[1:])
    return whole[: len(lines)].reshape(value.shape)


def joined_along(tiles, dim):
    dims = list(tiles.shape[1:])
    dims[dim] *= tiles.shape[0]
    return jnp.moveaxis(tiles, 0, dim).reshape(dims)


def collect(value, axis, dim):
    return joined_along(from_everyone(value, axis), dim)


def rms_scaled(values, gain_vec):
    floats = values.astype(jnp.float32)
    scaled = floats * lax.rsqrt(jnp.mean(floats * floats, axis=-1, keepdims=True) + epsilon)
    return (scaled * gain_vec).astype(jnp.bfloat16)


def on_device(
    stream,
    previous_state,
    mixer_norm_gain,
    query_matrix,
    key_matrix,
    value_matrix,
    output_gate_weight,
    decay_lower_factor,
    decay_upper_factor,
    forgetting_boost,
    head_norm_gain,
    output_matrix,
    mixture_norm_gain,
    expert_gate_weight,
    expert_up_weight,
    expert_down_weight,
    expert_index_table,
    expert_scores_within,
    group_probability,
):
    seq_count, model_width = stream.shape
    value_local = previous_state.shape[2]
    head_count = max(1, value_local // DV)
    head_width = min(value_local, DV)
    tp_index = lax.axis_index(TP)
    leading_head = tp_index * value_local // DV
    value_start = tp_index * value_local % DV
    key_column_span = head_count * KEY_CHANNELS
    normed = rms_scaled(stream, mixer_norm_gain)
    own_query = lax.dynamic_slice_in_dim(
        query_matrix, leading_head * KEY_CHANNELS, key_column_span, 1
    )
    own_key = lax.dynamic_slice_in_dim(key_matrix, leading_head * KEY_CHANNELS, key_column_span, 1)
    spread = lax.all_to_all(normed, "ep", split_axis=1, concat_axis=0, tiled=True)
    joined = jnp.concatenate([own_query, own_key, value_matrix, output_gate_weight], axis=1)
    summed = sent_and_summed(jnp.dot(spread, joined, preferred_element_type=jnp.float32), "ep", 0)
    query_sum = summed[:, :key_column_span]
    key_sum = summed[:, key_column_span : 2 * key_column_span]
    value_sum = summed[:, 2 * key_column_span : 2 * key_column_span + value_local]
    gate_sum = summed[:, 2 * key_column_span + value_local :]
    queries = (query_sum * KEY_CHANNELS ** (-0.5)).astype(jnp.bfloat16)
    key_rows = key_sum.astype(jnp.bfloat16)
    value_rows = value_sum.astype(jnp.bfloat16)
    gate_rows = gate_sum.astype(jnp.bfloat16)
    low_rank = jnp.dot(normed, decay_lower_factor, preferred_element_type=jnp.float32).astype(
        jnp.bfloat16
    )
    local_expand_matrix = lax.dynamic_slice_in_dim(
        decay_upper_factor, leading_head * KEY_CHANNELS, key_column_span, 1
    )
    forgetting_logit = jnp.dot(low_rank, local_expand_matrix, preferred_element_type=jnp.float32)
    request_boost = lax.dynamic_slice_in_dim(
        forgetting_boost, leading_head * KEY_CHANNELS, key_column_span, 1
    )
    forgetting_lograte = jax.nn.log_sigmoid(forgetting_logit) / forgetting_softness - request_boost
    factor = (
        jnp.exp(forgetting_lograte)
        .reshape(seq_count, head_count, KEY_CHANNELS)
        .transpose(0, 2, 1)[..., None]
    )
    state_four = previous_state.reshape(seq_count, KEY_CHANNELS, head_count, head_width)
    key_part = (
        key_rows.astype(jnp.float32)
        .reshape(seq_count, head_count, KEY_CHANNELS)
        .transpose(0, 2, 1)[..., None]
    )
    value_part = value_rows.astype(jnp.float32).reshape(seq_count, 1, head_count, head_width)
    updated = factor * state_four + key_part * value_part
    query_part = (
        queries.astype(jnp.float32).reshape(seq_count, head_count, KEY_CHANNELS).transpose(0, 2, 1)
    )
    readout = jnp.einsum("skh,skhv->shv", query_part, updated, precision=lax.Precision.HIGHEST)
    square_sums = jnp.sum(readout * readout, axis=-1)
    norm_table = lax.dynamic_update_slice(
        jnp.zeros((seq_count, HEAD_TOTAL), jnp.float32), square_sums, (jnp.int32(0), leading_head)
    )
    totals = of_everyone(norm_table, TP)
    own_totals = lax.dynamic_slice_in_dim(totals, leading_head, head_count, 1)
    mean_sq = own_totals[..., None] / DV
    own_gain = lax.dynamic_slice_in_dim(head_norm_gain, value_start, head_width, 0)
    gate_part = jax.nn.silu(
        gate_rows.astype(jnp.float32).reshape(seq_count, head_count, head_width)
    )
    gated_rows = (
        (readout * lax.rsqrt(mean_sq + epsilon) * own_gain * gate_part)
        .reshape(seq_count, value_local)
        .astype(jnp.bfloat16)
    )
    partial_out = jnp.dot(gated_rows, output_matrix, preferred_element_type=jnp.float32)
    mixer_sum = sum_by_parts(partial_out.astype(jnp.bfloat16), TP, (0, 1)).astype(jnp.float32)
    blended_tokens = (stream.astype(jnp.float32) + mixer_sum).astype(jnp.bfloat16)
    normed_two = rms_scaled(blended_tokens, mixture_norm_gain)
    ep_count = lax.axis_size("ep")
    local_experts = expert_gate_weight.shape[0]
    experts_all = ep_count * local_experts
    route_count = expert_index_table.shape[1]
    capacity = 2 * seq_count * route_count // experts_all
    slot_count = experts_all * capacity
    flat_ids = expert_index_table.reshape(seq_count * route_count)
    one_hot = (flat_ids[:, None] == jnp.arange(experts_all, dtype=jnp.int32)[None, :]).astype(
        jnp.int32
    )
    rank_in = jnp.sum(one_hot * (jnp.cumsum(one_hot, axis=0) - 1), axis=1)
    place_lookup = flat_ids * capacity + rank_in
    placing = (place_lookup[:, None] == jnp.arange(slot_count, dtype=jnp.int32)[None, :]).astype(
        jnp.float32
    )
    placing = placing.reshape(seq_count, route_count, slot_count)
    logit_exp = jnp.exp(expert_scores_within)
    weights = logit_exp / jnp.sum(logit_exp, axis=-1, keepdims=True) * group_probability[:, None]
    combine = jnp.einsum("sk,skc->sc", weights, placing, precision=lax.Precision.HIGHEST)
    dispatch = jnp.sum(placing, axis=1).astype(jnp.bfloat16)
    outgoing = jnp.einsum("sc,sd->cd", dispatch, normed_two, preferred_element_type=jnp.float32)
    outgoing = outgoing.astype(jnp.bfloat16).reshape(experts_all, capacity, model_width)
    width_local = expert_down_weight.shape[2]
    arrived = lax.all_to_all(outgoing, "ep", split_axis=0, concat_axis=0, tiled=True)
    held_slots = arrived.shape[1]
    grouped = arrived.reshape(ep_count, local_experts, held_slots, model_width)
    gate_pre = jnp.einsum(
        "sxcd,xfd->sxcf", grouped, expert_gate_weight, preferred_element_type=jnp.float32
    )
    up_pre = jnp.einsum(
        "sxcd,xfd->sxcf", grouped, expert_up_weight, preferred_element_type=jnp.float32
    )
    hidden = (jax.nn.silu(gate_pre) * up_pre).astype(jnp.bfloat16)
    outputs = jnp.einsum(
        "sxcf,xfd->sxcd",
        collect(hidden, TP, 3),
        expert_down_weight,
        preferred_element_type=jnp.float32,
    )
    ready_rows = outputs.astype(jnp.bfloat16).reshape(
        ep_count * local_experts, held_slots, width_local
    )
    returned = lax.all_to_all(ready_rows, "ep", split_axis=0, concat_axis=0, tiled=True)
    mixture = jnp.dot(
        combine,
        returned.reshape(slot_count, width_local).astype(jnp.float32),
        precision=lax.Precision.HIGHEST,
    )
    own_mixed = lax.dynamic_slice_in_dim(blended_tokens, tp_index * width_local, width_local, 1)
    new_stream = (own_mixed.astype(jnp.float32) + mixture).astype(jnp.bfloat16)
    return (new_stream, updated.reshape(seq_count, KEY_CHANNELS, value_local))


def solution(mesh):
    torus = Mesh(mesh.devices.reshape(mesh.shape["ep"], 8, 4), ("ep", "tp_0", "tp_1"))
    placed = (
        P("ep", None),
        P("ep", None, TP),
        P(),
        P("ep", None),
        P("ep", None),
        P("ep", TP),
        P("ep", TP),
        P(),
        P(),
        P("ep", None),
        P(),
        P(TP, None),
        P(),
        P("ep", TP, None),
        P("ep", TP, None),
        P("ep", None, TP),
        P("ep", None),
        P("ep", None),
        P("ep"),
    )
    return jax.shard_map(
        on_device,
        mesh=torus,
        in_specs=placed,
        out_specs=(P("ep", TP), P("ep", None, TP)),
        check_vma=False,
    )
```

profile of v0, /device:TPU:1, one launch (start us, length us, event | category | flops | bytes accessed | tf_op | source)
XLA Modules:
  0.0 357.2 jit_solution(10460707515304323342)
XLA Ops:
  7.2 1.2 fusion.9
  8.4 1.5 copy_bitcast_fusion
  9.8 20.4 %all-to-all-start = ((bf16[16,32,128]{2,0,1:T(8,128)(2,1)}), bf16[16,32,128]{2,0,1:T(8,128)(2,1)S(1)}, u32[]{:S(2)}, u32[]{:S(2)}) async-start(bf16[16,32,128]{2,0,1:T(8,128)(2,1)} %copy_bitcast_fusion), calls=%async_computation | async-start | bytes 262144 | tf_op jit(solution)/shard_map/all_to_all | solution.py:122
  30.3 0.8 constant_dynamic-slice_fusion
  31.1 15.0 %all-to-all-done = bf16[16,32,128]{2,0,1:T(8,128)(2,1)S(1)} async-done(((bf16[16,32,128]{2,0,1:T(8,128)(2,1)}), bf16[16,32,128]{2,0,1:T(8,128)(2,1)S(1)}, u32[]{:S(2)}, u32[]{:S(2)}) %all-to-all-start) | async-done | bytes 131104 | tf_op jit(solution)/shard_map/all_to_all | solution.py:122
  46.1 1.3 fusion.17
  47.4 5.3 %all-to-all-start.1 = ((f32[32,16,512]{2,1,0:T(8,128)}), f32[32,16,512]{2,1,0:T(8,128)S(1)}, u32[]{:S(2)}, u32[]{:S(2)}) async-start(f32[32,16,512]{2,1,0:T(8,128)} %fusion.17), calls=%async_computation.1 | async-start | bytes 2097152 | tf_op jit(solution)/shard_map/all_to_all | solution.py:24
  52.7 1.4 dynamic-slice
  54.1 1.4 dynamic-slice.2
  55.7 1.5 fusion.41
  57.3 51.2 %all-to-all-done.1 = f32[32,16,512]{2,1,0:T(8,128)S(1)} async-done(((f32[32,16,512]{2,1,0:T(8,128)}), f32[32,16,512]{2,1,0:T(8,128)S(1)}, u32[]{:S(2)}, u32[]{:S(2)}) %all-to-all-start.1) | async-done | bytes 1048608 | tf_op jit(solution)/shard_map/all_to_all | solution.py:24
  110.1 0.8 reshape.180
  110.8 9.7 %all-to-all-start.2 = ((f32[32,1,256]{2,1,0:T(1,128)}), f32[32,1,256]{2,1,0:T(1,128)S(1)}, u32[]{:S(2)}, u32[]{:S(2)}) async-start(f32[32,1,256]{2,1,0:T(1,128)} %reshape.180), calls=%async_computation.2 | async-start | bytes 65536 | tf_op jit(solution)/shard_map/all_to_all | solution.py:30
  120.9 0.7 copy-done.14
  122.4 6.9 %all-to-all-done.2 = f32[32,1,256]{2,1,0:T(1,128)S(1)} async-done(((f32[32,1,256]{2,1,0:T(1,128)}), f32[32,1,256]{2,1,0:T(1,128)S(1)}, u32[]{:S(2)}, u32[]{:S(2)}) %all-to-all-start.2) | async-done | bytes 32800 | tf_op jit(solution)/shard_map/all_to_all | solution.py:30
  129.8 0.7 reduce.4
  131.2 0.7 pad_bitcast_fusion
  132.0 70.2 %all-reduce.5.cloned.1.call-done = bf16[32,1,4096]{2,0,1:T(8,128)(2,1)} async-done(((bf16[32,1,4096]{2,0,1:T(8,128)(2,1)}), bf16[32,1,4096]{2,0,1:T(8,128)(2,1)}) %all-reduce.5.cloned.1.call-update) | async-done | bytes 262160
  202.3 0.9 constant_dynamic-slice_fusion.2
  203.1 12.7 %all-reduce.2 = bf16[4,1,4096]{2,0,1:T(4,128)(2,1)S(1)} all-reduce(bf16[4,1,4096]{2,0,1:T(4,128)(2,1)S(1)} %constant_dynamic-slice_fusion.2), channel_id=4, replica_groups=mesh['ep'=32,'tp_0'=8,'tp_1'=4] {'tp_1'}, use_global_device_ids=true, to_apply=%region_5.6.clone | all-reduce | flops 16384 | bytes 65536
  215.8 0.7 dynamic-slice_bitcast_fusion
  216.5 9.1 %all_gather.9 = bf16[4,1,4096]{2,1,0:T(2,128)(2,1)S(1)} all-gather(bf16[1,1,4096]{2,1,0:T(2,128)(2,1)S(1)} %dynamic-slice_bitcast_fusion), channel_id=1, replica_groups=mesh['ep'=32,'tp_0'=8,'tp_1'=4] {'tp_1'}, dimensions={0}, use_global_device_ids=true | all-gather | bytes 40960 | tf_op jit(solution)/shard_map/all_gather | solution.py:57
  225.6 19.0 %all-gather = bf16[32,1,4096]{2,1,0:T(2,128)(2,1)S(1)} all-gather(bf16[4,1,4096]{2,1,0:T(2,128)(2,1)S(1)} %all_gather.9), channel_id=2, replica_groups=mesh['ep'=32,'tp_0'=8,'tp_1'=4] {'tp_0'}, dimensions={0}, use_global_device_ids=true | all-gather | bytes 294912 | tf_op jit(solution)/shard_map/all_gather | solution.py:57
  245.9 1.1 reshape.154
  247.1 32.2 %all-to-all-start.3 = ((bf16[32,2,4096]{2,1,0:T(2,128)(2,1)}), bf16[32,2,4096]{2,1,0:T(2,128)(2,1)S(1)}, u32[]{:S(2)}, u32[]{:S(2)}) async-start(bf16[32,2,4096]{2,1,0:T(2,128)(2,1)} %reshape.154), calls=%async_computation.3 | async-start | bytes 1048576 | tf_op jit(solution)/shard_map/all_to_all | solution.py:204
  279.3 33.5 %all-to-all-done.3 = bf16[32,2,4096]{2,1,0:T(2,128)(2,1)S(1)} async-done(((bf16[32,2,4096]{2,1,0:T(2,128)(2,1)}), bf16[32,2,4096]{2,1,0:T(2,128)(2,1)S(1)}, u32[]{:S(2)}, u32[]{:S(2)}) %all-to-all-start.3) | async-done | bytes 524320 | tf_op jit(solution)/shard_map/all_to_all | solution.py:204
  313.8 1.2 reshape.182
  315.0 5.4 %all-to-all-start.4 = ((bf16[32,2,1024]{2,1,0:T(2,128)(2,1)}), bf16[32,2,1024]{2,1,0:T(2,128)(2,1)S(1)}, u32[]{:S(2)}, u32[]{:S(2)}) async-start(bf16[32,2,1024]{2,1,0:T(2,128)(2,1)} %reshape.182), calls=%async_computation.4 | async-start | bytes 262144 | tf_op jit(solution)/shard_map/all_to_all | solution.py:30
  320.6 9.2 %all-to-all-done.4 = bf16[32,2,1024]{2,1,0:T(2,128)(2,1)S(1)} async-done(((bf16[32,2,1024]{2,1,0:T(2,128)(2,1)}), bf16[32,2,1024]{2,1,0:T(2,128)(2,1)S(1)}, u32[]{:S(2)}, u32[]{:S(2)}) %all-to-all-start.4) | async-done | bytes 131104 | tf_op jit(solution)/shard_map/all_to_all | solution.py:30
  332.1 5.6 %all-to-all-start.5 = ((bf16[32,2,128]{2,1,0:T(2,128)(2,1)}), bf16[32,2,128]{2,1,0:T(2,128)(2,1)S(1)}, u32[]{:S(2)}, u32[]{:S(2)}) async-start(bf16[32,2,128]{2,1,0:T(2,128)(2,1)} %copy.91), calls=%async_computation.5 | async-start | bytes 32768 | tf_op jit(solution)/shard_map/all_to_all | solution.py:223
  338.0 11.7 %all-to-all-done.5 = bf16[32,2,128]{2,1,0:T(2,128)(2,1)S(1)} async-done(((bf16[32,2,128]{2,1,0:T(2,128)(2,1)}), bf16[32,2,128]{2,1,0:T(2,128)(2,1)S(1)}, u32[]{:S(2)}, u32[]{:S(2)}) %all-to-all-start.5) | async-done | bytes 16416 | tf_op jit(solution)/shard_map/all_to_all | solution.py:223
  349.7 0.7 fusion.3
  (76 shorter events, 8.7 us)
Async XLA Ops:
  7.2 123.7 %copy-start = (bf16[128,4096]{1,0:T(8,128)(2,1)S(1)}, bf16[128,4096]{1,0:T(8,128)(2,1)}, u32[]{:S(2)}) copy-start(bf16[128,4096]{1,0:T(8,128)(2,1)} %param.30) | copy-start | bytes 3145732
  7.2 1.2 copy-start.2
  9.8 36.3 %all-to-all-start = ((bf16[16,32,128]{2,0,1:T(8,128)(2,1)}), bf16[16,32,128]{2,0,1:T(8,128)(2,1)S(1)}, u32[]{:S(2)}, u32[]{:S(2)}) async-start(bf16[16,32,128]{2,0,1:T(8,128)(2,1)} %copy_bitcast_fusion), calls=%async_computation | async-start | bytes 262144 | tf_op jit(solution)/shard_map/all_to_all | solution.py:122
  30.3 15.8 %copy-start.6 = (bf16[128,128]{1,0:T(8,128)(2,1)S(1)}, bf16[128,128]{1,0:T(8,128)(2,1)}, u32[]{:S(2)}) copy-start(bf16[128,128]{1,0:T(8,128)(2,1)} %param.25) | copy-start | bytes 98308
  30.3 15.8 %copy-start.7 = (bf16[128,128]{1,0:T(8,128)(2,1)S(1)}, bf16[128,128]{1,0:T(8,128)(2,1)}, u32[]{:S(2)}) copy-start(bf16[128,128]{1,0:T(8,128)(2,1)} %param.24) | copy-start | bytes 98308
  47.4 8.1 %copy-start.9 = (s32[16,2]{0,1:T(2,128)S(1)}, s32[16,2]{0,1:T(2,128)}, u32[]{:S(2)}) copy-start(s32[16,2]{0,1:T(2,128)} %param.35) | copy-start | bytes 388
  47.4 8.4 %copy-start.5 = (f32[4096]{0:T(1024)S(1)}, f32[4096]{0:T(1024)}, u32[]{:S(2)}) copy-start(f32[4096]{0:T(1024)} %param.21) | copy-start | bytes 49156
  47.4 61.1 %all-to-all-start.1 = ((f32[32,16,512]{2,1,0:T(8,128)}), f32[32,16,512]{2,1,0:T(8,128)S(1)}, u32[]{:S(2)}, u32[]{:S(2)}) async-start(f32[32,16,512]{2,1,0:T(8,128)} %fusion.17), calls=%async_computation.1 | async-start | bytes 2097152 | tf_op jit(solution)/shard_map/all_to_all | solution.py:24
  52.7 55.9 %copy-start.3 = (f32[16,128,128]{2,1,0:T(8,128)S(1)}, f32[16,128,128]{2,1,0:T(8,128)}, u32[]{:S(2)}) copy-start(f32[16,128,128]{2,1,0:T(8,128)} %param.20) | copy-start | bytes 3145732
  109.2 21.4 %copy-start.1 = (f32[16,128,128]{2,1,0:T(8,128)}, f32[16,128,128]{2,1,0:T(8,128)S(1)}, u32[]{:S(2)}) copy-start(f32[16,128,128]{2,1,0:T(8,128)S(1)} %multiply_add_fusion) | copy-start | bytes 3145732
  110.8 18.4 %all-to-all-start.2 = ((f32[32,1,256]{2,1,0:T(1,128)}), f32[32,1,256]{2,1,0:T(1,128)S(1)}, u32[]{:S(2)}, u32[]{:S(2)}) async-start(f32[32,1,256]{2,1,0:T(1,128)} %reshape.180), calls=%async_computation.2 | async-start | bytes 65536 | tf_op jit(solution)/shard_map/all_to_all | solution.py:30
  120.5 81.7 %all-reduce.5.cloned.1.call-start = ((), (), s32[]{:S(2)}) async-start(), calls=%async_computation.6 | async-start | bytes 524288
  120.9 0.7 copy-start.14
  244.9 0.7 copy-start.8
  247.0 32.2 %copy-start.10 = (f32[16,2]{0,1:T(2,128)S(1)}, f32[16,2]{0,1:T(2,128)}, u32[]{:S(2)}) copy-start(f32[16,2]{0,1:T(2,128)} %param.36) | copy-start | bytes 388
  247.0 65.7 %copy-start.12 = (bf16[1,32,4096]{2,1,0:T(8,128)(2,1)S(1)}, bf16[1,32,4096]{2,1,0:T(8,128)(2,1)}, u32[]{:S(2)}) copy-start(bf16[1,32,4096]{2,1,0:T(8,128)(2,1)} %param.32) | copy-start | bytes 786436
  247.1 65.7 %all-to-all-start.3 = ((bf16[32,2,4096]{2,1,0:T(2,128)(2,1)}), bf16[32,2,4096]{2,1,0:T(2,128)(2,1)S(1)}, u32[]{:S(2)}, u32[]{:S(2)}) async-start(bf16[32,2,4096]{2,1,0:T(2,128)(2,1)} %reshape.154), calls=%async_computation.3 | async-start | bytes 1048576 | tf_op jit(solution)/shard_map/all_to_all | solution.py:204
  279.3 34.0 %copy-start.13 = (bf16[1,32,4096]{2,1,0:T(8,128)(2,1)S(1)}, bf16[1,32,4096]{2,1,0:T(8,128)(2,1)}, u32[]{:S(2)}) copy-start(bf16[1,32,4096]{2,1,0:T(8,128)(2,1)} %param.33) | copy-start | bytes 786436
  315.0 5.4 %copy-start.11 = (f32[16]{0:T(128)S(1)}, f32[16]{0:T(128)}, u32[]{:S(2)}) copy-start(f32[16]{0:T(128)} %param.37) | copy-start | bytes 196
  315.0 14.7 %all-to-all-start.4 = ((bf16[32,2,1024]{2,1,0:T(2,128)(2,1)}), bf16[32,2,1024]{2,1,0:T(2,128)(2,1)S(1)}, u32[]{:S(2)}, u32[]{:S(2)}) async-start(bf16[32,2,1024]{2,1,0:T(2,128)(2,1)} %reshape.182), calls=%async_computation.4 | async-start | bytes 262144 | tf_op jit(solution)/shard_map/all_to_all | solution.py:30
  330.4 1.0 copy-start.4
  332.1 17.5 %all-to-all-start.5 = ((bf16[32,2,128]{2,1,0:T(2,128)(2,1)}), bf16[32,2,128]{2,1,0:T(2,128)(2,1)S(1)}, u32[]{:S(2)}, u32[]{:S(2)}) async-start(bf16[32,2,128]{2,1,0:T(2,128)(2,1)} %copy.91), calls=%async_computation.5 | async-start | bytes 32768 | tf_op jit(solution)/shard_map/all_to_all | solution.py:223
Sparse Core Ops, SparseCore 0:
  132.0 70.1 all-reduce.4
where the time goes:
time: 358 us; the launch traced here: 357 us
  waiting for transfers between devices  198 us (55%)
  starting transfers between devices  78.6 us (22%)
  blocking collectives  40.7 us (11%)
  between operations  15.1 us (4%)
  local copies, waits for them, and re-layouts  13.9 us (4%)
  matrix products  6.01 us (2%)
  other arithmetic  5.17 us (1%)
    unnamed x2, waiting for transfers between devices  70.3 us
    all_to_all x1, waiting for transfers between devices, sent_and_summed(): lax.all_to_all(tiles, axis, split_axis=0, concat_axis=0, tiled=True)  51.2 us
    all_to_all x1, waiting for transfers between devices, on_device(): lax.all_to_all(outgoing, 'ep', split_axis=0, concat_axis=0, tiled=True)  33.5 us
    all_to_all x1, starting transfers between devices, on_device(): lax.all_to_all(outgoing, 'ep', split_axis=0, concat_axis=0, tiled=True)  32.2 us
    all_gather x2, blocking collectives, stacked_from(): tiles = lax.all_gather(tiles, axes[k])  28 us
    all_to_all x1, starting transfers between devices, on_device(): lax.all_to_all(normed, 'ep', split_axis=1, concat_axis=0, tiled=True)  20.4 us
    all_to_all x2, waiting for transfers between devices, from_everyone(): lax.all_to_all(jnp.broadcast_to(value[None], (length, *value.shape)), axi...  16 us
    all_to_all x2, starting transfers between devices, from_everyone(): lax.all_to_all(jnp.broadcast_to(value[None], (length, *value.shape)), axi...  15.1 us
  transfers between devices with their start and end apart: 7, of which 7 were waited for; matrix products, arithmetic and copies ran while one was open for 2% of the time, Pallas kernels for 0%

commit v1 on v0

v1 whole, which is shorter than its diff:
```python
import functools

import jax
import jax.numpy as jnp
from jax import lax
from jax.experimental import pallas as pl
from jax.experimental.pallas import tpu as pltpu
from jax.sharding import PartitionSpec as P

KEY_CHANNELS = 128
DV = 256
W = 128
NX = 4
EPSILON = 1e-06
SOFTNESS = 16.0
MESH = pl.DeviceIdType.MESH
F32 = jnp.float32
BF16 = jnp.bfloat16


def aligned(index, size):
    return pl.ds(pl.multiple_of(index * size, size), size)


def kernel(
    ec,
    tc,
    nx,
    cap,
    stream_h,
    state_h,
    gain1_h,
    query_h,
    key_h,
    value_h,
    gate_h,
    lower_h,
    upper_h,
    boost_h,
    hgain_h,
    wo_h,
    gain2_h,
    eg_h,
    eu_h,
    ed_h,
    ids_h,
    scores_h,
    prob_h,
    out_h,
    newstate_h,
    stream,
    state,
    gain1,
    wraw,
    wcat,
    lower,
    upper,
    boost,
    hgain,
    wo,
    gain2,
    egu,
    ed,
    ids,
    scores,
    prob,
    xin,
    pbuf,
    pin,
    ssb,
    obuf,
    oin,
    dbuf,
    rin,
    xg,
    w4,
    wdp,
    hin,
    rbuf,
    retin,
    ro,
    outv,
    factor_t,
    comb,
    disp,
    lsem,
    ssem,
    rsem,
    xsem,
    ysem,
):
    ep = lax.axis_index("ep")
    tp = lax.axis_index("tp")
    zc = ec // 2
    ny = tc // nx
    z = ep // 2
    core = ep % 2
    y = tp // nx
    x = tp % nx
    heads_before = tp * W // DV
    half = tp % (DV // W)
    seqs, width = stream.shape
    units = eg_h.shape[1]
    ff = units * tc
    slots = ec * cap

    barrier = pltpu.get_barrier_semaphore()

    def greet_ep(i, carry):
        pl.semaphore_signal(
            barrier, inc=1, device_id=((ep + i) % ec, tp), device_id_type=MESH
        )
        return carry

    def greet_tp(i, carry):
        pl.semaphore_signal(
            barrier, inc=1, device_id=(ep, (tp + i) % tc), device_id_type=MESH
        )
        return carry

    lax.fori_loop(1, ec, greet_ep, 0)
    lax.fori_loop(1, tc, greet_tp, 0)

    copies = {}

    def load(name, src, dst):
        cp = pltpu.make_async_copy(src, dst, lsem.at[len(copies)])
        cp.start()
        copies[name] = cp

    head_cols = aligned(heads_before, W)
    load("stream", stream_h, stream)
    load("gain1", gain1_h, gain1)
    load("wq", query_h.at[:, head_cols], wraw.at[:, pl.ds(0, W)])
    load("wk", key_h.at[:, head_cols], wraw.at[:, pl.ds(W, W)])
    load("wv", value_h, wraw.at[:, pl.ds(2 * W, W)])
    load("wg", gate_h, wraw.at[:, pl.ds(3 * W, W)])
    load("lower", lower_h, lower)
    load("upper", upper_h.at[:, head_cols], upper)
    load("boost", boost_h.at[:, head_cols], boost)
    load("state", state_h, state)
    load("ids", ids_h, ids)
    load("scores", scores_h, scores)
    load("prob", prob_h, prob)
    load("hgain", hgain_h, hgain)
    load("wo", wo_h, wo)
    load("gain2", gain2_h, gain2)
    load("eg", eg_h.at[0], egu.at[0])
    load("eu", eu_h.at[0], egu.at[1])
    load("ed", ed_h.at[0], ed)

    def arrive(*names):
        for name in names:
            copies[name].wait()

    def settle(ref, sem):
        pltpu.make_async_copy(ref, ref, sem).wait()

    arrive("gain1", "wq", "wk", "wv", "wg")
    gain_row = gain1[:, aligned(ep, W)]
    gain_col = jnp.transpose(jnp.broadcast_to(gain_row, (W, W)))
    gain_wide = jnp.concatenate([gain_col] * 4, axis=1)
    wcat[aligned(core, W), :] = (wraw[...].astype(F32) * gain_wide).astype(BF16)

    arrive("stream")
    rows = stream[...].astype(F32)
    scale1 = lax.rsqrt(jnp.mean(rows * rows, axis=1, keepdims=True) + EPSILON)
    normed = (rows * scale1 * gain1[...]).astype(BF16)

    pl.semaphore_wait(barrier, ec + tc - 2)

    def send(src, dst, sent, received, device):
        pltpu.make_async_remote_copy(
            src_ref=src,
            dst_ref=dst,
            send_sem=sent,
            recv_sem=received,
            device_id=device,
            device_id_type=MESH,
        ).start()

    half_rows = wcat.at[aligned(core, W)]
    send(half_rows, half_rows, ssem.at[0], rsem.at[0], (ep + 1 - 2 * core, tp))
    chip_width = 2 * W

    def send_x(to):
        send(
            stream.at[:, aligned(to, chip_width)],
            xin.at[aligned(z, seqs)],
            ssem.at[1],
            xsem.at[z],
            (to * 2 + core, tp),
        )

    send_x((z + zc // 2) % zc)

    def send_x_pair(i, carry):
        d = zc // 2 - i
        send_x((z + d) % zc)
        send_x((z + zc - d) % zc)
        return carry

    lax.fori_loop(1, zc // 2, send_x_pair, 0)

    arrive("lower", "upper", "boost")
    low = lax.dot_general(
        normed, lower[...], (((1,), (1,)), ((), ())), preferred_element_type=F32
    ).astype(BF16)
    logit = jnp.dot(low, upper[...], preferred_element_type=F32)
    lograte = jax.nn.log_sigmoid(logit) / SOFTNESS - boost[...]
    factor_t[...] = jnp.transpose(jnp.exp(lograte))

    arrive("ids", "scores", "prob")
    lane = lax.broadcasted_iota(jnp.int32, (seqs, slots), 1)
    mine = (lane // cap).astype(F32)
    diagonal = lax.broadcasted_iota(jnp.int32, (seqs, seqs), 0) == lax.broadcasted_iota(
        jnp.int32, (seqs, seqs), 1
    )

    def column(row):
        square = jnp.where(diagonal, jnp.broadcast_to(row, (seqs, seqs)), 0.0)
        return jnp.sum(square, axis=1, keepdims=True)

    first = jnp.where(column(ids[0:1, :].astype(F32)) == mine, 1.0, 0.0)
    second = jnp.where(column(ids[1:2, :].astype(F32)) == mine, 1.0, 0.0)
    either = first + second
    before = jnp.where(
        lax.broadcasted_iota(jnp.int32, (seqs, seqs), 1)
        < lax.broadcasted_iota(jnp.int32, (seqs, seqs), 0),
        1.0,
        0.0,
    )
    earlier = jnp.dot(
        before.astype(BF16), either.astype(BF16), preferred_element_type=F32
    )
    chosen = jnp.where(jnp.abs(earlier - (lane % cap).astype(F32)) < 0.5, either, 0.0)
    disp[...] = jnp.transpose(chosen).astype(BF16)
    raised = jnp.exp(scores[...])
    weights = raised / jnp.sum(raised, axis=0, keepdims=True) * prob[...]
    comb[...] = chosen * (first * column(weights[0:1, :]) + second * column(weights[1:2, :]))

    pltpu.make_async_remote_copy(
        src_ref=half_rows,
        dst_ref=wcat.at[aligned(1 - core, W)],
        send_sem=ssem.at[0],
        recv_sem=rsem.at[0],
        device_id=(ep + 1 - 2 * core, tp),
        device_id_type=MESH,
    ).wait()

    pin[aligned(z, seqs), :] = jnp.dot(
        stream[:, aligned(z, chip_width)], wcat[...], preferred_element_type=F32
    ).astype(BF16)

    def answer(to):
        settle(xin.at[aligned(to, seqs)], xsem.at[to])
        pbuf[aligned(to, seqs), :] = jnp.dot(
            xin[aligned(to, seqs), :], wcat[...], preferred_element_type=F32
        ).astype(BF16)
        send(
            pbuf.at[aligned(to, seqs)],
            pin.at[aligned(z, seqs)],
            ssem.at[2],
            rsem.at[1],
            (to * 2 + core, tp),
        )

    def answer_pair(d, carry):
        answer((z + d) % zc)
        answer((z + zc - d) % zc)
        return carry

    lax.fori_loop(1, zc // 2, answer_pair, 0)
    answer((z + zc // 2) % zc)

    arrive("state")
    for s in range(seqs):
        state[s] = state[s] * factor_t[:, s : s + 1]

    arrive("gain2", "eg", "eu")
    for which in range(2):
        scaled = (egu[which].astype(F32) * gain2[...]).astype(BF16)
        for copy in range(4):
            w4[pl.ds((which * 4 + copy) * units, units), :] = scaled
    arrive("ed")
    for g in range(4):
        for block in range(ff // units):
            source = block // 4 * 4 + (block % 4 - g) % 4
            wdp[g, pl.ds(block * units, units), :] = ed[pl.ds(source * units, units), :]
    arrive("hgain", "wo")

    settle(pin.at[pl.ds(0, (zc - 1) * seqs)], rsem.at[1])
    total = pin[pl.ds(0, seqs), :].astype(F32)
    for i in range(1, zc):
        total = total + pin[pl.ds(i * seqs, seqs), :].astype(F32)
    total = total * scale1

    query_t = jnp.transpose(total[:, :W] * KEY_CHANNELS**-0.5)
    key_t = jnp.transpose(total[:, W : 2 * W])
    value_rows = total[:, 2 * W : 3 * W]
    gate_rows = total[:, 3 * W :]
    for s in range(seqs):
        fresh = state[s] + key_t[:, s : s + 1] * value_rows[s : s + 1, :]
        state[s] = fresh
        ro[s : s + 1, :] = jnp.sum(query_t[:, s : s + 1] * fresh, axis=0, keepdims=True)
    readout = ro[...]
    squares = jnp.sum(readout * readout, axis=1, keepdims=True)
    ssb[0] = jnp.broadcast_to(squares, (seqs, W))
    partner = tp + 1 - 2 * half
    gated = (
        readout * hgain[:, aligned(half, W)] * (gate_rows * jax.nn.sigmoid(gate_rows))
    ).astype(BF16)
    exchange = pltpu.make_async_remote_copy(
        src_ref=ssb.at[0],
        dst_ref=ssb.at[1],
        send_sem=ssem.at[3],
        recv_sem=rsem.at[2],
        device_id=(ep, partner),
        device_id_type=MESH,
    )
    exchange.start()
    partial = jnp.dot(gated, wo[...], preferred_element_type=F32)
    store_state = pltpu.make_async_copy(state, newstate_h, lsem.at[len(copies)])
    store_state.start()
    exchange.wait()
    head_scale = lax.rsqrt((squares + ssb[1, :, 0:1]) / DV + EPSILON)
    obuf[...] = (partial * head_scale).astype(BF16)

    def send_o(i, carry):
        to = (tp + i) % tc
        send(obuf.at[:, aligned(to, W)], oin.at[tp], ssem.at[4], rsem.at[3], (ep, to))
        return carry

    lax.fori_loop(1, tc, send_o, 0)
    oin[tp] = obuf[:, aligned(tp, W)]
    settle(oin.at[pl.ds(0, tc - 1)], rsem.at[3])
    mixed = stream[:, aligned(tp, W)].astype(F32)
    summed = oin[0].astype(F32)
    for i in range(1, tc):
        summed = summed + oin[i].astype(F32)
    mixed = (mixed + summed).astype(BF16)

    dbuf[...] = jnp.dot(disp[...], mixed, preferred_element_type=F32).astype(BF16)

    def send_d(i, carry):
        to = (ep + i) % ec
        send(
            dbuf.at[aligned(to, cap)],
            rin.at[aligned(ep, cap)],
            ssem.at[5],
            rsem.at[4],
            (to, tp),
        )
        return carry

    lax.fori_loop(1, ec, send_d, 0)
    own = lax.broadcasted_iota(jnp.int32, (slots, W), 0) // cap == ep
    settle(rin.at[pl.ds(0, (ec - 1) * cap)], rsem.at[4])
    xg[tp] = jnp.where(own, dbuf[...].astype(F32), rin[...].astype(F32)).astype(BF16)

    def send_y(i, carry):
        to = ((y + i) % ny) * nx + x
        send(xg.at[tp], xg.at[tp], ssem.at[6], ysem.at[y], (ep, to))
        return carry

    lax.fori_loop(1, ny, send_y, 0)

    def pass_x(block):
        for i in range(1, nx):
            to = y * nx + (x + i) % nx
            send(xg.at[block], xg.at[block], ssem.at[7], rsem.at[5], (ep, to))

    pass_x(tp)

    def forward(i, carry):
        from_y = (y + i) % ny
        block = from_y * nx + x
        settle(xg.at[block], ysem.at[from_y])
        pass_x(block)
        return carry

    lax.fori_loop(1, ny, forward, 0)
    settle(xg.at[pl.ds(0, (nx - 1) * ny)], rsem.at[5])

    expert_rows = jnp.concatenate([xg[i] for i in range(tc)], axis=1)
    square = jnp.zeros((slots, W), F32)
    for i in range(tc):
        piece = xg[i].astype(F32)
        square = square + piece * piece
    scale2 = lax.rsqrt(jnp.sum(square, axis=1, keepdims=True) / width + EPSILON)
    both = lax.dot_general(
        expert_rows, w4[...], (((1,), (1,)), ((), ())), preferred_element_type=F32
    )
    gate_pre = both[:, : 4 * units] * scale2
    up_pre = both[:, 4 * units :] * scale2
    hidden = gate_pre * jax.nn.sigmoid(gate_pre) * up_pre
    group = slots // 4
    quarter = lax.broadcasted_iota(jnp.int32, (group, W), 1) // units
    tile = jnp.zeros((group, W), F32)
    for g in range(4):
        tile = jnp.where(
            quarter == (g + tp % 4) % 4, hidden[g * group : (g + 1) * group, :], tile
        )
    hin[tp] = tile.astype(BF16)

    def send_h(i, carry):
        to = (tp + i) % tc
        send(hin.at[tp], hin.at[tp], ssem.at[8], rsem.at[6], (ep, to))
        return carry

    lax.fori_loop(1, tc, send_h, 0)
    settle(hin.at[pl.ds(0, tc - 1)], rsem.at[6])

    for g in range(4):
        pieces = []
        for a in range(tc // 4):
            piece = hin[4 * a].astype(F32)
            for b in range(1, 4):
                piece = jnp.where(
                    quarter == (g + b) % 4, hin[4 * a + b].astype(F32), piece
                )
            pieces.append(piece.astype(BF16))
        rbuf[pl.ds(g * group, group), :] = jnp.dot(
            jnp.concatenate(pieces, axis=1), wdp[g], preferred_element_type=F32
        ).astype(BF16)

    def send_r(i, carry):
        to = (ep + i) % ec
        send(
            rbuf.at[aligned(to, cap)],
            retin.at[aligned(ep, cap)],
            ssem.at[9],
            rsem.at[7],
            (to, tp),
        )
        return carry

    lax.fori_loop(1, ec, send_r, 0)
    weight_high = comb[...].astype(BF16)
    weight_low = (comb[...] - weight_high.astype(F32)).astype(BF16)
    settle(retin.at[pl.ds(0, (ec - 1) * cap)], rsem.at[7])
    back = jnp.where(own, rbuf[...].astype(F32), retin[...].astype(F32)).astype(BF16)
    mixture = jnp.dot(weight_high, back, preferred_element_type=F32) + jnp.dot(
        weight_low, back, preferred_element_type=F32
    )
    outv[...] = (mixed.astype(F32) + mixture).astype(BF16)
    store_out = pltpu.make_async_copy(outv, out_h, lsem.at[len(copies) + 1])
    store_out.start()

    settle(xin.at[pl.ds(0, (zc - 1) * seqs)], ssem.at[1])
    settle(pbuf.at[pl.ds(0, (zc - 1) * seqs)], ssem.at[2])
    settle(oin.at[pl.ds(0, tc - 1)], ssem.at[4])
    settle(rin.at[pl.ds(0, (ec - 1) * cap)], ssem.at[5])
    settle(xg.at[pl.ds(0, ny - 1)], ssem.at[6])
    settle(xg.at[pl.ds(0, (nx - 1) * ny)], ssem.at[7])
    settle(hin.at[pl.ds(0, tc - 1)], ssem.at[8])
    settle(rin.at[pl.ds(0, (ec - 1) * cap)], ssem.at[9])
    store_state.wait()
    store_out.wait()


def on_device(ec, tc, nx, *args):
    (
        stream,
        previous_state,
        mixer_norm_gain,
        query_matrix,
        key_matrix,
        value_matrix,
        output_gate_weight,
        decay_lower_factor,
        decay_upper_factor,
        forgetting_boost,
        head_norm_gain,
        output_matrix,
        mixture_norm_gain,
        expert_gate_weight,
        expert_up_weight,
        expert_down_weight,
        expert_index_table,
        expert_scores_within,
        group_probability,
    ) = args
    seqs, width = stream.shape
    cap = 2 * seqs * expert_index_table.shape[1] // ec
    slots = ec * cap
    units = expert_gate_weight.shape[1]
    ff = expert_down_weight.shape[1]
    zc = ec // 2
    operands = (
        stream,
        previous_state,
        mixer_norm_gain.reshape(1, width),
        query_matrix,
        key_matrix,
        value_matrix,
        output_gate_weight,
        decay_lower_factor.T,
        decay_upper_factor,
        forgetting_boost,
        head_norm_gain.reshape(1, DV),
        output_matrix,
        mixture_norm_gain.reshape(1, width),
        expert_gate_weight,
        expert_up_weight,
        expert_down_weight,
        expert_index_table.T,
        expert_scores_within.T,
        group_probability.reshape(1, seqs),
    )
    v = pltpu.VMEM
    scratch = [
        v((seqs, width), BF16),
        v(previous_state.shape, F32),
        v((1, width), F32),
        v((W, 4 * W), BF16),
        v((2 * W, 4 * W), BF16),
        v(decay_lower_factor.shape[::-1], BF16),
        v((decay_upper_factor.shape[0], W), BF16),
        v((seqs, W), F32),
        v((1, DV), F32),
        v(output_matrix.shape, BF16),
        v((1, width), F32),
        v((2, units, width), BF16),
        v((ff, W), BF16),
        v(expert_index_table.shape[::-1], jnp.int32),
        v(expert_scores_within.shape[::-1], F32),
        v((1, seqs), F32),
        v((zc * seqs, 2 * W), BF16),
        v((zc * seqs, 4 * W), BF16),
        v((zc * seqs, 4 * W), BF16),
        v((2, seqs, W), F32),
        v((seqs, width), BF16),
        v((tc, seqs, W), BF16),
        v((slots, W), BF16),
        v((slots, W), BF16),
        v((tc, slots, W), BF16),
        v((8 * units, width), BF16),
        v((4, ff, W), BF16),
        v((tc, slots // 4, W), BF16),
        v((slots, W), BF16),
        v((slots, W), BF16),
        v((seqs, W), F32),
        v((seqs, W), BF16),
        v((W, seqs), F32),
        v((seqs, slots), F32),
        v((slots, seqs), BF16),
        pltpu.SemaphoreType.DMA((21,)),
        pltpu.SemaphoreType.DMA((10,)),
        pltpu.SemaphoreType.DMA((8,)),
        pltpu.SemaphoreType.DMA((zc,)),
        pltpu.SemaphoreType.DMA((tc // nx,)),
    ]
    hbm = pl.BlockSpec(memory_space=pltpu.HBM)
    return pl.pallas_call(
        functools.partial(kernel, ec, tc, nx, cap),
        out_shape=(
            jax.ShapeDtypeStruct((seqs, W), BF16),
            jax.ShapeDtypeStruct(previous_state.shape, F32),
        ),
        in_specs=[hbm] * len(operands),
        out_specs=(hbm, hbm),
        scratch_shapes=scratch,
        compiler_params=pltpu.CompilerParams(
            collective_id=0, has_side_effects=True, vmem_limit_bytes=67043328
        ),
        name="layer",
    )(*operands)


def solution(mesh):
    ec, tc = mesh.shape["ep"], mesh.shape["tp"]
    placed = (
        P("ep", None),
        P("ep", None, "tp"),
        P(),
        P("ep", None),
        P("ep", None),
        P("ep", "tp"),
        P("ep", "tp"),
        P(),
        P(),
        P("ep", None),
        P(),
        P("tp", None),
        P(),
        P("ep", "tp", None),
        P("ep", "tp", None),
        P("ep", None, "tp"),
        P("ep", None),
        P("ep", None),
        P("ep"),
    )
    return jax.shard_map(
        functools.partial(on_device, ec, tc, min(NX, tc // 2)),
        mesh=mesh,
        in_specs=placed,
        out_specs=(P("ep", "tp"), P("ep", None, "tp")),
        check_vma=False,
    )
```

time: 358 us -> 101 us (0.28)
  waiting for transfers between devices: 198 us -> 0 us
  Pallas kernels: 0 us -> 96.2 us
  starting transfers between devices: 78.6 us -> 0 us
  blocking collectives: 40.7 us -> 0 us
  between operations: 15.1 us -> 0.65 us
  local copies, waits for them, and re-layouts: 13.9 us -> 3.57 us
  matrix products: 6.01 us -> 0 us
  other arithmetic: 5.17 us -> 0 us
    all_to_all x6 -> x0, waiting for transfers between devices: 127 us -> none  [the longest x1 51.2 us: sent_and_summed(): lax.all_to_all(tiles, axis, split_axis=0, concat_axis=0, tiled=True)]
    pallas_call x0 -> x1, Pallas kernels: none -> 96.2 us  [on_device(): pl.pallas_call(functools.partial(kernel, ec, tc, nx, cap), out_shape=(jax...]
    all_to_all x6 -> x0, starting transfers between devices: 78.6 us -> none  [the longest x1 32.2 us: on_device(): lax.all_to_all(outgoing, 'ep', split_axis=0, concat_axis=0, tiled=True)]
    unnamed x2 -> x0, waiting for transfers between devices: 70.3 us -> none
    all_gather x2 -> x0, blocking collectives: 28 us -> none  [stacked_from(): tiles = lax.all_gather(tiles, axes[k])]
    unnamed x1 -> x0, blocking collectives: 12.7 us -> none
    dot_general x10 -> x0, matrix products: 6.01 us -> none  [the longest x1 1.52 us: on_device(): jnp.dot(low_rank, local_expand_matrix, preferred_element_type=jnp.float32)]
    unnamed x39 -> x2, local copies, waits for them, and re-layouts: 7.65 us -> 3.57 us
  transfers between devices with their start and end apart: 7 -> 0, of which waited for: 7 -> 0; matrix products, arithmetic and copies ran while one was open for 2% -> 0% of each run, Pallas kernels for 0% -> 0%
where the time goes in v1:
time: 101 us; the launch traced here: 100 us
  Pallas kernels  96.2 us (95%)
  local copies, waits for them, and re-layouts  3.57 us (4%)
    pallas_call x1, Pallas kernels, on_device(): pl.pallas_call(functools.partial(kernel, ec, tc, nx, cap), out_shape=(jax...  96.2 us
    unnamed x2, local copies, waits for them, and re-layouts  3.57 us

profile of v1, /device:TPU:1, one launch (start us, length us, event | category | flops | bytes accessed | tf_op | source)
XLA Modules:
  0.0 100.4 jit_solution(3803186517556214764)
XLA Ops:
  0.6 96.2 %layer.1 = (bf16[16,128]{1,0:T(8,128)(2,1)}, f32[16,128,128]{2,1,0:T(8,128)}) custom-call(bf16[16,4096]{1,0:T(8,128)(2,1)} %stream_h.1, f32[16,128,128]{2,1,0:T(8,128)} %state_h.1, f32[1,4096]{1,0:T(1,128)} %bitcast.8, bf16[128,2048]{1,0:T(8,128)(2,1)} %query_h.1, bf16[128,2048]{1,0:T(8,128)(2,1)} %key_h.1, bf16[128,128]{1,0:T(8,128)(2,1)} %value_h.1, ...), custom_call_target="tpu_custom_call" | custom-call | tf_op jit(solution)/shard_map/layer/pallas_call | solution.py:555
  96.8 1.3 %copy.23 = bf16[16,128]{1,0:T(8,128)(2,1)} copy(bf16[16,128]{1,0:T(8,128)(2,1)} %get-tuple-element.4) | data formatting | bytes 8192
  98.1 2.3 %copy.24 = f32[16,128,128]{2,1,0:T(8,128)} copy(f32[16,128,128]{2,1,0:T(8,128)} %get-tuple-element.5) | data formatting | bytes 2097152

commit v2 on v1

--- a/solution.py
+++ b/solution.py
@@ -67,6 +67,9 @@
     xin,
     pbuf,
     pin,
+    qbuf,
+    qin,
+    qkb,
     ssb,
     obuf,
     oin,
@@ -87,7 +90,7 @@
     ssem,
     rsem,
     xsem,
-    ysem,
+    bsem,
 ):
     ep = lax.axis_index("ep")
     tp = lax.axis_index("tp")
@@ -159,8 +162,13 @@
     arrive("gain1", "wq", "wk", "wv", "wg")
     gain_row = gain1[:, aligned(ep, W)]
     gain_col = jnp.transpose(jnp.broadcast_to(gain_row, (W, W)))
-    gain_wide = jnp.concatenate([gain_col] * 4, axis=1)
-    wcat[aligned(core, W), :] = (wraw[...].astype(F32) * gain_wide).astype(BF16)
+    first_half = half == 0
+    shared = jnp.where(
+        first_half, wraw[:, :W].astype(F32), wraw[:, W : 2 * W].astype(F32)
+    )
+    wcat[aligned(core, W), :W] = (shared * gain_col).astype(BF16)
+    gain_wide = jnp.concatenate([gain_col] * 2, axis=1)
+    wcat[aligned(core, W), W:] = (wraw[:, 2 * W :].astype(F32) * gain_wide).astype(BF16)
 
     arrive("stream")
     rows = stream[...].astype(F32)
@@ -248,15 +256,47 @@
         device_id_type=MESH,
     ).wait()
 
-    pin[aligned(z, seqs), :] = jnp.dot(
-        stream[:, aligned(z, chip_width)], wcat[...], preferred_element_type=F32
+    xin[aligned(z, seqs), :] = stream[:, aligned(z, chip_width)]
+
+    qin[aligned(z, seqs), :] = jnp.dot(
+        xin[aligned(z, seqs), :], wcat[:, :W], preferred_element_type=F32
     ).astype(BF16)
 
-    def answer(to):
-        settle(xin.at[aligned(to, seqs)], xsem.at[to])
-        pbuf[aligned(to, seqs), :] = jnp.dot(
-            xin[aligned(to, seqs), :], wcat[...], preferred_element_type=F32
-        ).astype(BF16)
+    def send_q(to):
+        send(
+            qbuf.at[aligned(to, seqs)],
+            qin.at[aligned(z, seqs)],
+            ssem.at[10],
+            rsem.at[8],
+            (to * 2 + core, tp),
+        )
+
+    def answer_pair(d, carry):
+        above = (z + d) % zc
+        below = (z + zc - d) % zc
+        settle(xin.at[aligned(above, seqs)], xsem.at[above])
+        settle(xin.at[aligned(below, seqs)], xsem.at[below])
+        pair = jnp.concatenate(
+            [xin[aligned(above, seqs), :], xin[aligned(below, seqs), :]], axis=0
+        )
+        sums = jnp.dot(pair, wcat[:, :W], preferred_element_type=F32).astype(BF16)
+        qbuf[aligned(above, seqs), :] = sums[:seqs]
+        qbuf[aligned(below, seqs), :] = sums[seqs:]
+        send_q(above)
+        send_q(below)
+        return carry
+
+    lax.fori_loop(1, zc // 2, answer_pair, 0)
+    across = (z + zc // 2) % zc
+    settle(xin.at[aligned(across, seqs)], xsem.at[across])
+    qbuf[aligned(across, seqs), :] = jnp.dot(
+        xin[aligned(across, seqs), :], wcat[:, :W], preferred_element_type=F32
+    ).astype(BF16)
+    send_q(across)
+
+    pbuf[...] = jnp.dot(xin[...], wcat[:, W:], preferred_element_type=F32).astype(BF16)
+
+    def send_p(to):
         send(
             pbuf.at[aligned(to, seqs)],
             pin.at[aligned(z, seqs)],
@@ -265,13 +305,16 @@
             (to * 2 + core, tp),
         )
 
-    def answer_pair(d, carry):
-        answer((z + d) % zc)
-        answer((z + zc - d) % zc)
-        return carry
-
-    lax.fori_loop(1, zc // 2, answer_pair, 0)
-    answer((z + zc // 2) % zc)
+    send_p(across)
+
+    def send_p_pair(i, carry):
+        d = zc // 2 - i
+        send_p((z + d) % zc)
+        send_p((z + zc - d) % zc)
+        return carry
+
+    lax.fori_loop(1, zc // 2, send_p_pair, 0)
+    pin[aligned(z, seqs), :] = pbuf[aligned(z, seqs), :]
 
     arrive("state")
     for s in range(seqs):
@@ -289,16 +332,35 @@
             wdp[g, pl.ds(block * units, units), :] = ed[pl.ds(source * units, units), :]
     arrive("hgain", "wo")
 
+    settle(qin.at[pl.ds(0, (zc - 1) * seqs)], rsem.at[8])
+    own_sum = qin[pl.ds(0, seqs), :].astype(F32)
+    for i in range(1, zc):
+        own_sum = own_sum + qin[pl.ds(i * seqs, seqs), :].astype(F32)
+    partner = tp + 1 - 2 * half
+    qkb[0] = own_sum * scale1
+    swap = pltpu.make_async_remote_copy(
+        src_ref=qkb.at[0],
+        dst_ref=qkb.at[1],
+        send_sem=ssem.at[11],
+        recv_sem=rsem.at[9],
+        device_id=(ep, partner),
+        device_id_type=MESH,
+    )
+    swap.start()
+
     settle(pin.at[pl.ds(0, (zc - 1) * seqs)], rsem.at[1])
     total = pin[pl.ds(0, seqs), :].astype(F32)
     for i in range(1, zc):
         total = total + pin[pl.ds(i * seqs, seqs), :].astype(F32)
     total = total * scale1
-
-    query_t = jnp.transpose(total[:, :W] * KEY_CHANNELS**-0.5)
-    key_t = jnp.transpose(total[:, W : 2 * W])
-    value_rows = total[:, 2 * W : 3 * W]
-    gate_rows = total[:, 3 * W :]
+    swap.wait()
+
+    query_rows = jnp.where(first_half, qkb[0], qkb[1])
+    key_rows = jnp.where(first_half, qkb[1], qkb[0])
+    query_t = jnp.transpose(query_rows * KEY_CHANNELS**-0.5)
+    key_t = jnp.transpose(key_rows)
+    value_rows = total[:, :W]
+    gate_rows = total[:, W:]
     for s in range(seqs):
         fresh = state[s] + key_t[:, s : s + 1] * value_rows[s : s + 1, :]
         state[s] = fresh
@@ -306,7 +368,6 @@
     readout = ro[...]
     squares = jnp.sum(readout * readout, axis=1, keepdims=True)
     ssb[0] = jnp.broadcast_to(squares, (seqs, W))
-    partner = tp + 1 - 2 * half
     gated = (
         readout * hgain[:, aligned(half, W)] * (gate_rows * jax.nn.sigmoid(gate_rows))
     ).astype(BF16)
@@ -360,7 +421,7 @@
 
     def send_y(i, carry):
         to = ((y + i) % ny) * nx + x
-        send(xg.at[tp], xg.at[tp], ssem.at[6], ysem.at[y], (ep, to))
+        send(xg.at[tp], xg.at[tp], ssem.at[6], bsem.at[tp], (ep, to))
         return carry
 
     lax.fori_loop(1, ny, send_y, 0)
@@ -368,29 +429,46 @@
     def pass_x(block):
         for i in range(1, nx):
             to = y * nx + (x + i) % nx
-            send(xg.at[block], xg.at[block], ssem.at[7], rsem.at[5], (ep, to))
+            send(xg.at[block], xg.at[block], ssem.at[7], bsem.at[block], (ep, to))
 
     pass_x(tp)
 
+    def from_row(i):
+        return (y + ny + (2 * (i % 2) - 1) * ((i + 1) // 2)) % ny
+
     def forward(i, carry):
-        from_y = (y + i) % ny
-        block = from_y * nx + x
-        settle(xg.at[block], ysem.at[from_y])
+        block = from_row(i) * nx + x
+        settle(xg.at[block], bsem.at[block])
         pass_x(block)
         return carry
 
     lax.fori_loop(1, ny, forward, 0)
-    settle(xg.at[pl.ds(0, (nx - 1) * ny)], rsem.at[5])
-
-    expert_rows = jnp.concatenate([xg[i] for i in range(tc)], axis=1)
-    square = jnp.zeros((slots, W), F32)
-    for i in range(tc):
-        piece = xg[i].astype(F32)
-        square = square + piece * piece
+
+    def products(i, carry):
+        both, square = carry
+        row = from_row(i) * nx
+        for k in range(1, nx):
+            block = row + (x + k) % nx
+            settle(xg.at[block], bsem.at[block])
+        pieces = [xg[row + k] for k in range(nx)]
+        for piece in pieces:
+            floats = piece.astype(F32)
+            square = square + floats * floats
+        both = both + lax.dot_general(
+            jnp.concatenate(pieces, axis=1),
+            w4[:, aligned(from_row(i), nx * W)],
+            (((1,), (1,)), ((), ())),
+            preferred_element_type=F32,
+        )
+        return both, square
+
+    both, square = lax.fori_loop(
+        0,
+        ny,
+        products,
+        (jnp.zeros((slots, 8 * units), F32), jnp.zeros((slots, W), F32)),
+    )
     scale2 = lax.rsqrt(jnp.sum(square, axis=1, keepdims=True) / width + EPSILON)
-    both = lax.dot_general(
-        expert_rows, w4[...], (((1,), (1,)), ((), ())), preferred_element_type=F32
-    )
     gate_pre = both[:, : 4 * units] * scale2
     up_pre = both[:, 4 * units :] * scale2
     hidden = gate_pre * jax.nn.sigmoid(gate_pre) * up_pre
@@ -449,6 +527,7 @@
 
     settle(xin.at[pl.ds(0, (zc - 1) * seqs)], ssem.at[1])
     settle(pbuf.at[pl.ds(0, (zc - 1) * seqs)], ssem.at[2])
+    settle(qbuf.at[pl.ds(0, (zc - 1) * seqs)], ssem.at[10])
     settle(oin.at[pl.ds(0, tc - 1)], ssem.at[4])
     settle(rin.at[pl.ds(0, (ec - 1) * cap)], ssem.at[5])
     settle(xg.at[pl.ds(0, ny - 1)], ssem.at[6])
@@ -457,6 +536,28 @@
     settle(rin.at[pl.ds(0, (ec - 1) * cap)], ssem.at[9])
     store_state.wait()
     store_out.wait()
+
+
+def hand_over(out_h, state_h, out_to, state_to, outv, state, sem):
+    pieces = 8
+    rows = state.shape[0] // pieces
+    ins = [pltpu.make_async_copy(out_h, outv, sem.at[0])]
+    outs = [pltpu.make_async_copy(outv, out_to, sem.at[1])]
+    for i in range(pieces):
+        part = pl.ds(i * rows, rows)
+        ins.append(
+            pltpu.make_async_copy(state_h.at[part], state.at[part], sem.at[2 + 2 * i])
+        )
+        outs.append(
+            pltpu.make_async_copy(state.at[part], state_to.at[part], sem.at[3 + 2 * i])
+        )
+    for copy in ins:
+        copy.start()
+    for arriving, leaving in zip(ins, outs):
+        arriving.wait()
+        leaving.start()
+    for copy in outs:
+        copy.wait()
 
 
 def on_device(ec, tc, nx, *args):
@@ -514,7 +615,7 @@
         v(previous_state.shape, F32),
         v((1, width), F32),
         v((W, 4 * W), BF16),
-        v((2 * W, 4 * W), BF16),
+        v((2 * W, 3 * W), BF16),
         v(decay_lower_factor.shape[::-1], BF16),
         v((decay_upper_factor.shape[0], W), BF16),
         v((seqs, W), F32),
@@ -527,8 +628,11 @@
         v(expert_scores_within.shape[::-1], F32),
         v((1, seqs), F32),
         v((zc * seqs, 2 * W), BF16),
-        v((zc * seqs, 4 * W), BF16),
-        v((zc * seqs, 4 * W), BF16),
+        v((zc * seqs, 2 * W), BF16),
+        v((zc * seqs, 2 * W), BF16),
+        v((zc * seqs, W), BF16),
+        v((zc * seqs, W), BF16),
+        v((2, seqs, W), F32),
         v((2, seqs, W), F32),
         v((seqs, width), BF16),
         v((tc, seqs, W), BF16),
@@ -546,13 +650,13 @@
         v((seqs, slots), F32),
         v((slots, seqs), BF16),
         pltpu.SemaphoreType.DMA((21,)),
+        pltpu.SemaphoreType.DMA((12,)),
         pltpu.SemaphoreType.DMA((10,)),
-        pltpu.SemaphoreType.DMA((8,)),
         pltpu.SemaphoreType.DMA((zc,)),
-        pltpu.SemaphoreType.DMA((tc // nx,)),
+        pltpu.SemaphoreType.DMA((tc,)),
     ]
     hbm = pl.BlockSpec(memory_space=pltpu.HBM)
-    return pl.pallas_call(
+    results = pl.pallas_call(
         functools.partial(kernel, ec, tc, nx, cap),
         out_shape=(
             jax.ShapeDtypeStruct((seqs, W), BF16),
@@ -566,6 +670,19 @@
         ),
         name="layer",
     )(*operands)
+    return pl.pallas_call(
+        hand_over,
+        out_shape=[jax.ShapeDtypeStruct(a.shape, a.dtype) for a in results],
+        in_specs=[hbm] * 2,
+        out_specs=[hbm] * 2,
+        scratch_shapes=[
+            v((seqs, W), BF16),
+            v(previous_state.shape, F32),
+            pltpu.SemaphoreType.DMA((18,)),
+        ],
+        compiler_params=pltpu.CompilerParams(vmem_limit_bytes=67043328),
+        name="hand_over",
+    )(*results)
 
 
 def solution(mesh):

time: 101 us -> 93.8 us (0.929)
  local copies, waits for them, and re-layouts: 3.57 us -> 0 us
  Pallas kernels: 96.2 us -> 93 us
    pallas_call x1, Pallas kernels: 96.2 us -> 90.9 us  [on_device(): pl.pallas_call(functools.partial(kernel, ec, tc, nx, cap), out_shape=(jax...]
    unnamed x2 -> x0, local copies, waits for them, and re-layouts: 3.57 us -> none
    pallas_call x0 -> x1, Pallas kernels: none -> 2.11 us  [on_device(): pl.pallas_call(hand_over, out_shape=[jax.ShapeDtypeStruct(a.shape, a.dtyp...]
where the time goes in v2:
time: 93.8 us; the launch traced here: 93.7 us
  Pallas kernels  93 us (99%)
    pallas_call x1, Pallas kernels, on_device(): pl.pallas_call(functools.partial(kernel, ec, tc, nx, cap), out_shape=(jax...  90.9 us
    pallas_call x1, Pallas kernels, on_device(): pl.pallas_call(hand_over, out_shape=[jax.ShapeDtypeStruct(a.shape, a.dtyp...  2.11 us

profile of v2, /device:TPU:1, one launch (start us, length us, event | category | flops | bytes accessed | tf_op | source)
XLA Modules:
  0.0 93.7 jit_solution(9501064020250180786)
XLA Ops:
  0.6 90.9 %layer.1 = (bf16[16,128]{1,0:T(8,128)(2,1)}, f32[16,128,128]{2,1,0:T(8,128)}) custom-call(bf16[16,4096]{1,0:T(8,128)(2,1)} %stream_h.1, f32[16,128,128]{2,1,0:T(8,128)} %state_h.1, f32[1,4096]{1,0:T(1,128)} %bitcast.8, bf16[128,2048]{1,0:T(8,128)(2,1)} %query_h.1, bf16[128,2048]{1,0:T(8,128)(2,1)} %key_h.1, bf16[128,128]{1,0:T(8,128)(2,1)} %value_h.1, ...), custom_call_target="tpu_custom_call" | custom-call | tf_op jit(solution)/shard_map/layer/pallas_call | solution.py:659
  91.5 2.1 %hand_over.1 = (bf16[16,128]{1,0:T(8,128)(2,1)}, f32[16,128,128]{2,1,0:T(8,128)}) custom-call(bf16[16,128]{1,0:T(8,128)(2,1)} %get-tuple-element.4.out_h, f32[16,128,128]{2,1,0:T(8,128)} %get-tuple-element.5.state_h), custom_call_target="tpu_custom_call" | custom-call | tf_op jit(solution)/shard_map/hand_over/pallas_call | solution.py:673

commit v3 on v2

--- a/solution.py
+++ b/solution.py
@@ -109,20 +109,44 @@
 
     barrier = pltpu.get_barrier_semaphore()
 
-    def greet_ep(i, carry):
-        pl.semaphore_signal(
-            barrier, inc=1, device_id=((ep + i) % ec, tp), device_id_type=MESH
-        )
-        return carry
-
-    def greet_tp(i, carry):
-        pl.semaphore_signal(
-            barrier, inc=1, device_id=(ep, (tp + i) % tc), device_id_type=MESH
-        )
-        return carry
-
-    lax.fori_loop(1, ec, greet_ep, 0)
-    lax.fori_loop(1, tc, greet_tp, 0)
+    def every_ep(put):
+        def chip(to):
+            put(to * 2 + 1 - core)
+            put(to * 2 + core)
+
+        def pair(i, carry):
+            d = zc // 2 - i
+            chip(lax.rem(z + d, zc))
+            chip(lax.rem(z + zc - d, zc))
+            return carry
+
+        chip(lax.rem(z + zc // 2, zc))
+        lax.fori_loop(1, zc // 2, pair, 0)
+        put(ep + 1 - 2 * core)
+
+    offsets = sorted(range(nx), key=lambda o: -min(o, nx - o))
+    columns = [lax.rem(x + o, nx) for o in offsets]
+
+    def every_tp(put):
+        def row(to):
+            for column in columns:
+                put(to * nx + column)
+
+        def pair(i, carry):
+            d = ny // 2 - i
+            row(lax.rem(y + d, ny))
+            row(lax.rem(y + ny - d, ny))
+            return carry
+
+        row(lax.rem(y + ny // 2, ny))
+        lax.fori_loop(1, ny // 2, pair, 0)
+        for column in columns[:-1]:
+            put(y * nx + column)
+
+    def greet(device):
+        pl.semaphore_signal(barrier, inc=1, device_id=device, device_id_type=MESH)
+
+    every_ep(lambda to: greet((to, tp)))
 
     copies = {}
 
@@ -151,6 +175,8 @@
     load("eg", eg_h.at[0], egu.at[0])
     load("eu", eu_h.at[0], egu.at[1])
     load("ed", ed_h.at[0], ed)
+
+    every_tp(lambda to: greet((ep, to)))
 
     def arrive(*names):
         for name in names:
@@ -387,12 +413,10 @@
     head_scale = lax.rsqrt((squares + ssb[1, :, 0:1]) / DV + EPSILON)
     obuf[...] = (partial * head_scale).astype(BF16)
 
-    def send_o(i, carry):
-        to = (tp + i) % tc
+    def send_o(to):
         send(obuf.at[:, aligned(to, W)], oin.at[tp], ssem.at[4], rsem.at[3], (ep, to))
-        return carry
-
-    lax.fori_loop(1, tc, send_o, 0)
+
+    every_tp(send_o)
     oin[tp] = obuf[:, aligned(tp, W)]
     settle(oin.at[pl.ds(0, tc - 1)], rsem.at[3])
     mixed = stream[:, aligned(tp, W)].astype(F32)
@@ -403,8 +427,7 @@
 
     dbuf[...] = jnp.dot(disp[...], mixed, preferred_element_type=F32).astype(BF16)
 
-    def send_d(i, carry):
-        to = (ep + i) % ec
+    def send_d(to):
         send(
             dbuf.at[aligned(to, cap)],
             rin.at[aligned(ep, cap)],
@@ -412,15 +435,17 @@
             rsem.at[4],
             (to, tp),
         )
-        return carry
-
-    lax.fori_loop(1, ec, send_d, 0)
+
+    every_ep(send_d)
     own = lax.broadcasted_iota(jnp.int32, (slots, W), 0) // cap == ep
     settle(rin.at[pl.ds(0, (ec - 1) * cap)], rsem.at[4])
     xg[tp] = jnp.where(own, dbuf[...].astype(F32), rin[...].astype(F32)).astype(BF16)
 
+    def from_row(i):
+        return (y + ny + (2 * (i % 2) - 1) * ((i + 1) // 2)) % ny
+
     def send_y(i, carry):
-        to = ((y + i) % ny) * nx + x
+        to = from_row(i) * nx + x
         send(xg.at[tp], xg.at[tp], ssem.at[6], bsem.at[tp], (ep, to))
         return carry
 
@@ -432,9 +457,6 @@
             send(xg.at[block], xg.at[block], ssem.at[7], bsem.at[block], (ep, to))
 
     pass_x(tp)
-
-    def from_row(i):
-        return (y + ny + (2 * (i % 2) - 1) * ((i + 1) // 2)) % ny
 
     def forward(i, carry):
         block = from_row(i) * nx + x
@@ -481,12 +503,10 @@
         )
     hin[tp] = tile.astype(BF16)
 
-    def send_h(i, carry):
-        to = (tp + i) % tc
+    def send_h(to):
         send(hin.at[tp], hin.at[tp], ssem.at[8], rsem.at[6], (ep, to))
-        return carry
-
-    lax.fori_loop(1, tc, send_h, 0)
+
+    every_tp(send_h)
     settle(hin.at[pl.ds(0, tc - 1)], rsem.at[6])
 
     for g in range(4):
@@ -502,8 +522,7 @@
             jnp.concatenate(pieces, axis=1), wdp[g], preferred_element_type=F32
         ).astype(BF16)
 
-    def send_r(i, carry):
-        to = (ep + i) % ec
+    def send_r(to):
         send(
             rbuf.at[aligned(to, cap)],
             retin.at[aligned(ep, cap)],
@@ -511,9 +530,8 @@
             rsem.at[7],
             (to, tp),
         )
-        return carry
-
-    lax.fori_loop(1, ec, send_r, 0)
+
+    every_ep(send_r)
     weight_high = comb[...].astype(BF16)
     weight_low = (comb[...] - weight_high.astype(F32)).astype(BF16)
     settle(retin.at[pl.ds(0, (ec - 1) * cap)], rsem.at[7])

time: 93.8 us -> 92 us (0.981)
  Pallas kernels: 93 us -> 91.1 us
    pallas_call x1, Pallas kernels: 90.9 us -> 89 us  [on_device(): pl.pallas_call(functools.partial(kernel, ec, tc, nx, cap), out_shape=(jax...]
where the time goes in v3:
time: 92 us; the launch traced here: 91.8 us
  Pallas kernels  91.1 us (99%)
    pallas_call x1, Pallas kernels, on_device(): pl.pallas_call(functools.partial(kernel, ec, tc, nx, cap), out_shape=(jax...  89 us
    pallas_call x1, Pallas kernels, on_device(): pl.pallas_call(hand_over, out_shape=[jax.ShapeDtypeStruct(a.shape, a.dtyp...  2.11 us

profile of v3, /device:TPU:1, one launch (start us, length us, event | category | flops | bytes accessed | tf_op | source)
XLA Modules:
  0.0 91.8 jit_solution(921251628084423095)
XLA Ops:
  0.6 89.0 %layer.1 = (bf16[16,128]{1,0:T(8,128)(2,1)}, f32[16,128,128]{2,1,0:T(8,128)}) custom-call(bf16[16,4096]{1,0:T(8,128)(2,1)} %stream_h.1, f32[16,128,128]{2,1,0:T(8,128)} %state_h.1, f32[1,4096]{1,0:T(1,128)} %bitcast.8, bf16[128,2048]{1,0:T(8,128)(2,1)} %query_h.1, bf16[128,2048]{1,0:T(8,128)(2,1)} %key_h.1, bf16[128,128]{1,0:T(8,128)(2,1)} %value_h.1, ...), custom_call_target="tpu_custom_call" | custom-call | tf_op jit(solution)/shard_map/layer/pallas_call | solution.py:677
  89.7 2.1 %hand_over.1 = (bf16[16,128]{1,0:T(8,128)(2,1)}, f32[16,128,128]{2,1,0:T(8,128)}) custom-call(bf16[16,128]{1,0:T(8,128)(2,1)} %get-tuple-element.4.out_h, f32[16,128,128]{2,1,0:T(8,128)} %get-tuple-element.5.state_h), custom_call_target="tpu_custom_call" | custom-call | tf_op jit(solution)/shard_map/hand_over/pallas_call | solution.py:691
